TPU v7x, 32 devices: a whole 2x2x4 slice. The times are simulated.
32 devices in a mesh: ep: 16 (over z, y, x), tp: 2 (over core).
Axes of the slice: x: 2, y: 2, z: 4, core: 2. Of those that a mesh axis runs over, the one named last changes fastest.
Arguments:
- tokens: bfloat16 [512, 3072], P('ep'), may hold values from -6 to 6
- carried: float32 [512, 96, 128], P('ep', 'tp'), may hold values from -4 to 4
- decay_rate: float32 [96, 64], P('tp'), may hold values from 0.02 to 20
- frequency: float32 [96, 64], P('tp'), may hold values from 0 to 200
- log_step: float32 [96], P('tp'), may hold values from -4.6 to 0
- in_map: bfloat16 [96, 128, 16], P('tp'), may hold values from -1 to 1
- out_map: bfloat16 [96, 16, 128], P('tp'), may hold values from -0.5 to 0.5
- skip_gain: float32 [1536], P('tp'), may hold values from -4 to 4
- norm_gain: float32 [3072], replicated, may hold values from 0.1 to 1.9
- w_in: bfloat16 [3072, 1536], P(None, 'tp'), may hold values from -0.109375 to 0.109375
- w_out: bfloat16 [1536, 3072], P('tp'), may hold values from -0.15625 to 0.15625
- expert_gain: float32 [3072], replicated, may hold values from 0.1 to 1.9
- route_ids: int32 [512, 2], P('ep'), may hold values from 0 to 7, all different within a row; in each aligned block of 32 rows (0 to 31, 32 to 63, ...) at most 16 rows name the same one
- route_logit: float32 [512, 2], P('ep'), may hold values from -6 to 6
- w_gate: bfloat16 [3072, 43008], P(None, ('ep', 'tp')), may hold values from -0.109375 to 0.109375
- w_up: bfloat16 [3072, 43008], P(None, ('ep', 'tp')), may hold values from -0.109375 to 0.109375
- w_down: bfloat16 [43008, 3072], P(('ep', 'tp')), may hold values from -0.078125 to 0.078125
Outputs:
- new_tokens: bfloat16 [512, 3072], P('ep', 'tp')
- new_carried: float32 [512, 96, 128], P('ep', 'tp')
Inputs may be any that keep to these rules, and one draw needn't show every extreme that they name: `route_ids`: each row names 2 different experts; within each aligned block of 32 rows (the rows of one index of ep) no expert is named by more than 16 rows, a bound that some block reaches.
All inputs are finite; a program needn't handle non-finite values.
Results may differ from a plain program's by a relative error of at most 0.014.
Values may be sent and summed in bfloat16 or wider, within the bound.
A program may use at most 128 MiB of HBM per device.

v0:
```python
import jax
import jax.numpy as jnp
from jax import lax
from jax.sharding import PartitionSpec as P

EXPERTS = 8
TOP = 2
CAP = 16


def normalize(rows, gain):
    wide = rows.astype(jnp.float32)
    scaled = wide * lax.rsqrt(jnp.mean(wide * wide, axis=-1, keepdims=True) + 1e-06)
    return (scaled * gain).astype(jnp.bfloat16)


def state_update(drive, carried, decay_rate, frequency, log_step, in_map, out_map, skip_gain):
    count_rows, width = drive.shape
    groups, half = decay_rate.shape
    channels = width // groups
    step_size = jnp.exp(log_step)[:, None]
    magnitude = jnp.exp(-decay_rate * step_size)
    real_decay = magnitude * jnp.cos(frequency * step_size)
    imag_decay = magnitude * jnp.sin(frequency * step_size)
    denom = decay_rate * decay_rate + frequency * frequency
    real_less = real_decay - 1.0
    real_factor = (-real_less * decay_rate + imag_decay * frequency) / denom
    imag_factor = (-imag_decay * decay_rate - real_less * frequency) / denom
    grouped_drive = drive.reshape(count_rows, groups, channels)
    projected = jnp.einsum(
        "sgh,gqh->sgq", grouped_drive, in_map, preferred_element_type=jnp.float32
    )
    real_in = projected[..., :half]
    imag_in = projected[..., half:]
    real_push = real_factor * real_in - imag_factor * imag_in
    imag_push = real_factor * imag_in + imag_factor * real_in
    real_old = carried[..., :half]
    imag_old = carried[..., half:]
    real_new = real_decay * real_old - imag_decay * imag_old + real_push
    imag_new = real_decay * imag_old + imag_decay * real_old + imag_push
    joined = jnp.concatenate([real_new, -imag_new], axis=-1)
    reading = jnp.einsum(
        "sgq,ghq->sgh", joined, out_map.astype(jnp.float32), precision=lax.Precision.HIGHEST
    )
    total = reading.reshape(count_rows, width) + skip_gain * drive.astype(jnp.float32)
    activated = jax.nn.gelu(total).astype(jnp.bfloat16)
    return (activated, jnp.concatenate([real_new, imag_new], axis=-1))


def route_weights(route_logit):
    first = jax.nn.sigmoid(route_logit[:, 0] - route_logit[:, 1])
    second = jax.nn.sigmoid(route_logit[:, 1] - route_logit[:, 0])
    return jnp.stack([first, second], axis=1)


def per_device(
    tokens,
    carried,
    decay_rate,
    frequency,
    log_step,
    in_map,
    out_map,
    skip_gain,
    norm_gain,
    w_in,
    w_out,
    expert_gain,
    route_ids,
    route_logit,
    w_gate,
    w_up,
    w_down,
):
    count_rows, model_width = tokens.shape
    normed = normalize(tokens, norm_gain)
    drive = jnp.dot(normed, w_in, preferred_element_type=jnp.float32).astype(jnp.bfloat16)
    activated, new_carried = state_update(
        drive, carried, decay_rate, frequency, log_step, in_map, out_map, skip_gain
    )
    partial_value = jnp.dot(activated, w_out, preferred_element_type=jnp.float32).astype(
        jnp.bfloat16
    )
    summed = lax.psum(partial_value.astype(jnp.float32).astype(jnp.bfloat16), "tp").astype(
        jnp.float32
    )
    mixed = (tokens.astype(jnp.float32) + summed).astype(jnp.bfloat16)
    expert_in = normalize(mixed, expert_gain)
    weights = route_weights(route_logit)
    ep_count = lax.axis_size("ep")
    group_size = ep_count // EXPERTS
    expert_ids = jnp.arange(EXPERTS, dtype=jnp.int32)
    routes_flat = route_ids.reshape(-1)
    weights_flat = weights.reshape(-1)
    onehot = (routes_flat[:, None] == expert_ids[None, :]).astype(jnp.int32)
    earlier = jnp.cumsum(onehot, axis=0) - onehot
    slot_index = jnp.sum(earlier * onehot, axis=1)
    position = routes_flat * CAP + slot_index
    placement = (jnp.arange(EXPERTS * CAP, dtype=jnp.int32)[:, None] == position[None, :]).astype(
        jnp.float32
    )
    per_token = placement.reshape(EXPERTS * CAP, count_rows, TOP).sum(axis=2)
    packed = jnp.dot(per_token.astype(jnp.bfloat16), expert_in, preferred_element_type=jnp.float32)
    packed = packed.astype(jnp.bfloat16).reshape(EXPERTS, CAP, model_width)
    outgoing = jnp.repeat(packed, group_size, axis=0)
    received = lax.all_to_all(outgoing, "ep", split_axis=0, concat_axis=0, tiled=True)
    sources, slots, features = received.shape
    rows = received.reshape(sources * slots, features)
    gated = jnp.dot(rows, w_gate, preferred_element_type=jnp.float32)
    upward = jnp.dot(rows, w_up, preferred_element_type=jnp.float32)
    hidden = (jax.nn.silu(gated) * upward).astype(jnp.bfloat16)
    produced = jnp.dot(hidden, w_down, preferred_element_type=jnp.float32)
    produced = produced.reshape(sources, slots, features)
    halves = lax.psum_scatter(
        produced.astype(jnp.bfloat16), "tp", scatter_dimension=2, tiled=True
    ).astype(jnp.float32)
    returned = lax.all_to_all(
        halves.astype(jnp.bfloat16), "ep", split_axis=0, concat_axis=0, tiled=True
    ).astype(halves.dtype)
    per_expert = returned.reshape(EXPERTS, group_size, CAP, -1).sum(axis=1)
    per_expert = per_expert.reshape(EXPERTS * CAP, -1)
    weighing = (
        (placement * weights_flat[None, :]).reshape(EXPERTS * CAP, count_rows, TOP).sum(axis=2)
    )
    expert_sum = jnp.dot(
        weighing.T, per_expert, preferred_element_type=jnp.float32, precision=lax.Precision.HIGHEST
    )
    half_width = model_width // lax.axis_size("tp")
    column_start = lax.axis_index("tp") * half_width
    own_mixed = lax.dynamic_slice_in_dim(mixed, column_start, half_width, 1)
    new_tokens = (own_mixed.astype(jnp.float32) + expert_sum).astype(jnp.bfloat16)
    return (new_tokens, new_carried)


def solution(mesh):
    return jax.shard_map(
        per_device,
        mesh=mesh,
        in_specs=(
            P("ep", None),
            P("ep", "tp", None),
            P("tp", None),
            P("tp", None),
            P("tp"),
            P("tp", None, None),
            P("tp", None, None),
            P("tp"),
            P(),
            P(None, "tp"),
            P("tp", None),
            P(),
            P("ep", None),
            P("ep", None),
            P(None, ("ep", "tp")),
            P(None, ("ep", "tp")),
            P(("ep", "tp"), None),
        ),
        out_specs=(P("ep", "tp"), P("ep", "tp", None)),
        check_vma=False,
    )
```

profile of v0, /device:TPU:0, one launch (start us, length us, event | category | flops | bytes accessed | tf_op | source)
XLA Modules:
  0.0 152.5 jit_solution(15072366406423989595)
XLA Ops:
  7.2 0.0 copy-start
  7.2 0.0 all-reduce.2.cloned.1.call-start
  7.2 0.7 exp.18
  7.9 1.1 fusion.9
  9.0 0.0 copy-start.1
  9.0 3.5 %convolution_convert_fusion.3 = bf16[32,768]{1,0:T(8,128)(2,1)S(1)} fusion(bf16[3072,768]{1,0:T(8,128)(2,1)} %param.26, bf16[32,3072]{1,0:T(8,128)(2,1)} %param.17, f32[3072]{0:T(1024)} %param.25, f32[32]{0:T(128)S(1)} %add_rsqrt_fusion.1), kind=kOutput, calls=%fused_computation.9 | convolution fusion | flops 151412736 | bytes 4976768 | tf_op jit(solution)/shard_map/dot_general | solution.py:77
  12.5 0.2 copy.48
  12.7 0.0 copy-start.4
  12.7 0.0 copy-start.5
  12.7 0.3 fusion.44
  13.0 0.3 convolution_bitcast_fusion
  13.3 0.1 copy-done.4
  13.4 0.0 copy-done.5
  13.4 0.2 cosine_multiply_fusion
  13.6 0.0 copy-start.3
  13.6 0.8 fusion.43
  14.4 0.0 copy-start.8
  14.4 0.1 copy-done.3
  14.6 0.8 fusion.2
  15.4 0.1 copy.49
  15.5 0.0 copy-start.9
  15.6 0.0 copy-start.6
  15.6 4.0 %convolution_convert_fusion.2 = bf16[32,3072]{1,0:T(8,128)(2,1)} fusion(bf16[768,3072]{1,0:T(8,128)(2,1)} %param.27, f32[32,768]{1,0:T(8,128)S(1)} %copy.49, bf16[32,768]{1,0:T(8,128)(2,1)S(1)} %convolution_convert_fusion.3, f32[768]{0:T(1024)S(1)} %copy-done.8), kind=kOutput, calls=%fused_computation.2 | convolution fusion | flops 151388160 | bytes 5065728 | tf_op jit(solution)/shard_map/dot_general | solution.py:81
  19.6 0.0 all-reduce.2.cloned.1.call-update
  19.6 0.0 reduce-scatter.2.cloned.1.call-start
  19.7 0.1 copy.50
  19.8 0.1 eq.31
  19.9 0.1 fusion.33
  19.9 0.1 reduce_window_sum.11
  20.0 0.2 select_reduce_fusion.1
  20.2 0.1 reduce_sum.58
  20.3 0.1 copy.51
  20.4 0.1 convert_reduce_fusion.1
  20.5 20.0 %all-reduce.2.cloned.1.call-done = bf16[32,3072]{1,0:T(8,128)(2,1)} async-done(((bf16[32,3072]{1,0:T(8,128)(2,1)}), bf16[32,3072]{1,0:T(8,128)(2,1)}) %all-reduce.2.cloned.1.call-update) | async-done | bytes 196624 | tf_op jit(solution)/shard_map/psum | solution.py:84
  40.5 1.1 fusion.6
  41.6 0.4 convolution_convert_fusion.1
  42.1 0.2 broadcast_in_dim.2
  42.3 44.6 %all_to_all.10 = bf16[16,16,3072]{2,1,0:T(8,128)(2,1)S(1)} all-to-all(bf16[16,16,3072]{2,1,0:T(8,128)(2,1)S(1)} %bitcast.27), channel_id=1, replica_groups=mesh['ep'=16,'tp'=2] {'ep'}, dimensions={0} | all-to-all | bytes 3145728 | tf_op jit(solution)/shard_map/all_to_all | solution.py:106
  86.9 6.8 %fusion.45 = f32[256,1344]{0,1:T(8,128)} fusion(bf16[256,3072]{1,0:T(8,128)(2,1)S(1)} %bitcast.31, bf16[3072,1344]{0,1:T(8,128)(2,1)} %param.31), kind=kOutput, calls=%fused_computation.74 | convolution fusion | flops 2113929216 | bytes 11206656 | tf_op jit(solution)/shard_map/dot_general | solution.py:109
  93.6 16.3 %convolution_convert_fusion = bf16[256,3072]{1,0:T(8,128)(2,1)} fusion(bf16[1344,3072]{1,0:T(8,128)(2,1)} %param.33, bf16[256,3072]{1,0:T(8,128)(2,1)S(1)} %bitcast.32, bf16[3072,1344]{0,1:T(8,128)(2,1)} %param.32, f32[256,1344]{0,1:T(8,128)} %fusion.45), kind=kOutput, calls=%fused_computation | convolution fusion | flops 4230709248 | bytes 21037056 | tf_op jit(solution)/shard_map/dot_general | solution.py:112
  110.0 0.0 reduce-scatter.2.cloned.1.call-update
  110.0 7.5 %reduce-scatter.2.cloned.1.call-done = bf16[16,16,1536]{2,1,0:T(8,128)(2,1)} async-done(((bf16[16,16,3072]{2,1,0:T(8,128)(2,1)}), bf16[16,16,1536]{2,1,0:T(8,128)(2,1)}) %reduce-scatter.2.cloned.1.call-update) | async-done | bytes 786448 | tf_op jit(solution)/shard_map/reduce_scatter | solution.py:114
  117.4 6.9 %all-to-all-start.1 = ((bf16[16,16,1536]{2,1,0:T(8,128)(2,1)}), bf16[16,16,1536]{2,1,0:T(8,128)(2,1)S(1)}, u32[]{:S(2)}, u32[]{:S(2)}) async-start(bf16[16,16,1536]{2,1,0:T(8,128)(2,1)} %reduce-scatter.2.cloned.1.call-done), calls=%async_computation.2 | async-start | bytes 1572864 | tf_op jit(solution)/shard_map/all_to_all | solution.py:117
  124.3 0.3 pad_maximum_fusion
  124.6 1.3 copy.52
  126.0 18.4 %all-to-all-done.1 = bf16[16,16,1536]{2,1,0:T(8,128)(2,1)S(1)} async-done(((bf16[16,16,1536]{2,1,0:T(8,128)(2,1)}), bf16[16,16,1536]{2,1,0:T(8,128)(2,1)S(1)}, u32[]{:S(2)}, u32[]{:S(2)}) %all-to-all-start.1) | async-done | bytes 786464 | tf_op jit(solution)/shard_map/all_to_all | solution.py:117
  144.3 0.1 convert_reduce_fusion
  144.5 1.2 fusion.1
  (14 shorter events, 0.1 us)
Async XLA Ops:
  7.2 5.8 %copy-start = (bf16[48,128,16]{1,2,0:T(8,128)(2,1)S(1)}, bf16[48,128,16]{1,2,0:T(8,128)(2,1)}, u32[]{:S(2)}) copy-start(bf16[48,128,16]{1,2,0:T(8,128)(2,1)} %param.22) | copy-start | bytes 589828
  7.2 33.3 %all-reduce.2.cloned.1.call-start = ((), (), s32[]{:S(2)}) async-start(), calls=%async_computation.3 | async-start | bytes 393216 | tf_op jit(solution)/shard_map/psum | solution.py:84
  9.0 3.7 %copy-start.1 = (f32[32,48,128]{2,1,0:T(8,128)S(1)}, f32[32,48,128]{2,1,0:T(8,128)}, u32[]{:S(2)}) copy-start(f32[32,48,128]{2,1,0:T(8,128)} %param.18) | copy-start | bytes 2359300
  12.7 0.7 copy-start.4
  12.7 0.7 copy-start.5
  13.6 0.9 copy-start.3
  14.4 1.1 copy-start.8
  15.5 4.1 %copy-start.9 = (f32[32,2]{0,1:T(2,128)S(1)}, f32[32,2]{0,1:T(2,128)}, u32[]{:S(2)}) copy-start(f32[32,2]{0,1:T(2,128)} %param.30) | copy-start | bytes 772
  15.6 4.1 %copy-start.7 = (s32[32,2]{0,1:T(2,128)S(1)}, s32[32,2]{0,1:T(2,128)}, u32[]{:S(2)}) copy-start(s32[32,2]{0,1:T(2,128)} %param.29) | copy-start | bytes 772
  15.6 25.0 %copy-start.2 = (bf16[32,3072]{1,0:T(8,128)(2,1)S(1)}, bf16[32,3072]{1,0:T(8,128)(2,1)}, u32[]{:S(2)}) copy-start(bf16[32,3072]{1,0:T(8,128)(2,1)} %param.17) | copy-start | bytes 589828
  15.6 26.1 %copy-start.6 = (f32[3072]{0:T(1024)S(1)}, f32[3072]{0:T(1024)}, u32[]{:S(2)}) copy-start(f32[3072]{0:T(1024)} %param.28) | copy-start | bytes 36868
  19.6 97.9 %reduce-scatter.2.cloned.1.call-start = ((), (), s32[]{:S(2)}) async-start(), calls=%async_computation.4 | async-start | bytes 2359296 | tf_op jit(solution)/shard_map/reduce_scatter | solution.py:114
  117.4 26.9 %all-to-all-start.1 = ((bf16[16,16,1536]{2,1,0:T(8,128)(2,1)}), bf16[16,16,1536]{2,1,0:T(8,128)(2,1)S(1)}, u32[]{:S(2)}, u32[]{:S(2)}) async-start(bf16[16,16,1536]{2,1,0:T(8,128)(2,1)} %reduce-scatter.2.cloned.1.call-done), calls=%async_computation.2 | async-start | bytes 1572864 | tf_op jit(solution)/shard_map/all_to_all | solution.py:117
Sparse Core Ops, SparseCore 0:
  19.7 20.7 all-reduce.1
  110.1 7.2 reduce-scatter.1
where the time goes:
time: 153 us; the launch traced here: 152 us
  waiting for transfers between devices  45.9 us (30%)
  blocking collectives  44.6 us (29%)
  matrix products  33.3 us (22%)
  between operations  14.3 us (9%)
  starting transfers between devices  6.98 us (5%)
  other arithmetic  4.03 us (3%)
  local copies, waits for them, and re-layouts  3.47 us (2%)
    all_to_all x1, blocking collectives, per_device(): lax.all_to_all(outgoing, 'ep', split_axis=0, concat_axis=0, tiled=True)  44.6 us
    psum x1, waiting for transfers between devices, per_device(): lax.psum(partial_value.astype(jnp.float32).astype(jnp.bfloat16), 'tp')  20 us
    all_to_all x1, waiting for transfers between devices, per_device(): lax.all_to_all(halves.astype(jnp.bfloat16), 'ep', split_axis=0, concat_ax...  18.4 us
    dot_general x1, matrix products, per_device(): produced = jnp.dot(hidden, w_down, preferred_element_type=jnp.float32)  16.3 us
    reduce_scatter x1, waiting for transfers between devices, per_device(): lax.psum_scatter(produced.astype(jnp.bfloat16), 'tp', scatter_dimension=2...  7.46 us
    all_to_all x1, starting transfers between devices, per_device(): lax.all_to_all(halves.astype(jnp.bfloat16), 'ep', split_axis=0, concat_ax...  6.9 us
    dot_general x1, matrix products, per_device(): gated = jnp.dot(rows, w_gate, preferred_element_type=jnp.float32)  6.77 us
    dot_general x1, matrix products, per_device(): jnp.dot(activated, w_out, preferred_element_type=jnp.float32)  3.96 us
  transfers between devices with their start and end apart: 3, of which 3 were waited for; matrix products, arithmetic and copies ran while one was open for 2% of the time, Pallas kernels for 0%

commit v1 on v0

--- a/solution.py
+++ b/solution.py
@@ -6,6 +6,10 @@
 EXPERTS = 8
 TOP = 2
 CAP = 16
+
+
+def choose_shards_for(local_array):
+    return jnp.sum(lax.all_gather(local_array, "tp"), axis=0)
 
 
 def normalize(rows, gain):
@@ -81,7 +85,7 @@
     partial_value = jnp.dot(activated, w_out, preferred_element_type=jnp.float32).astype(
         jnp.bfloat16
     )
-    summed = lax.psum(partial_value.astype(jnp.float32).astype(jnp.bfloat16), "tp").astype(
+    summed = choose_shards_for(partial_value.astype(jnp.float32).astype(jnp.bfloat16)).astype(
         jnp.float32
     )
     mixed = (tokens.astype(jnp.float32) + summed).astype(jnp.bfloat16)

time: 153 us -> 137 us (0.90)
  waiting for transfers between devices: 45.9 us -> 25.8 us
  blocking collectives: 44.6 us -> 48.2 us
    psum x1 -> x0, waiting for transfers between devices: 20 us -> none  [per_device(): lax.psum(partial_value.astype(jnp.float32).astype(jnp.bfloat16), 'tp')]
    all_gather x0 -> x1, blocking collectives: none -> 2.35 us  [choose_shards_for(): return jnp.sum(lax.all_gather(local_array, 'tp'), axis=0)]
  transfers between devices with their start and end apart: 3 -> 2, of which waited for: 3 -> 2; matrix products, arithmetic and copies ran while one was open for 2% -> 1% of each run, Pallas kernels for 0% -> 0%
where the time goes in v1:
time: 137 us
  blocking collectives  48.2 us (35%)
  matrix products  32.6 us (24%)
  waiting for transfers between devices  25.8 us (19%)
  between operations  14.2 us (10%)
  starting transfers between devices  6.95 us (5%)
  other arithmetic  4.67 us (3%)
  local copies, waits for them, and re-layouts  4.13 us (3%)
    all_to_all x1, blocking collectives, per_device(): lax.all_to_all(outgoing, 'ep', split_axis=0, concat_axis=0, tiled=True)  45.9 us
    all_to_all x1, waiting for transfers between devices, per_device(): lax.all_to_all(halves.astype(jnp.bfloat16), 'ep', split_axis=0, concat_ax...  18.4 us
    dot_general x1, matrix products, per_device(): produced = jnp.dot(hidden, w_down, preferred_element_type=jnp.float32)  16.3 us
    reduce_scatter x1, waiting for transfers between devices, per_device(): lax.psum_scatter(produced.astype(jnp.bfloat16), 'tp', scatter_dimension=2...  7.43 us
    all_to_all x1, starting transfers between devices, per_device(): lax.all_to_all(halves.astype(jnp.bfloat16), 'ep', split_axis=0, concat_ax...  6.91 us
    dot_general x1, matrix products, per_device(): gated = jnp.dot(rows, w_gate, preferred_element_type=jnp.float32)  6.77 us
    dot_general x1, matrix products, per_device(): jnp.dot(normed, w_in, preferred_element_type=jnp.float32)  3.47 us
    dot_general x1, matrix products, per_device(): jnp.dot(activated, w_out, preferred_element_type=jnp.float32)  3.26 us
  transfers between devices with their start and end apart: 2, of which 2 were waited for; matrix products, arithmetic and copies ran while one was open for 1% of the time, Pallas kernels for 0%

profile of v1, /device:TPU:0, one launch (start us, length us, event | category | flops | bytes accessed | tf_op | source)
XLA Modules:
  0.0 136.6 jit_solution(17342804729848064801)
XLA Ops:
  7.2 0.0 copy-start
  7.2 0.0 reduce-scatter.2.cloned.1.call-start
  7.2 0.7 exp.18
  7.9 1.1 fusion.9
  9.0 0.8 add_divide_fusion.1
  9.8 0.8 copy.50
  10.6 0.1 eq.31
  10.7 0.1 fusion.33
  10.7 0.1 reduce_window_sum.11
  10.8 0.2 select_reduce_fusion.1
  11.0 0.1 reduce_sum.71
  11.1 0.1 copy.51
  11.2 0.7 multiply_add_fusion.1
  11.9 3.5 %convolution_convert_fusion.3 = bf16[32,768]{1,0:T(8,128)(2,1)S(1)} fusion(bf16[3072,768]{1,0:T(8,128)(2,1)} %param.26, bf16[32,3072]{1,0:T(8,128)(2,1)} %param.17, f32[3072]{0:T(1024)} %param.25, f32[32]{0:T(128)S(1)} %add_rsqrt_fusion.1), kind=kOutput, calls=%fused_computation.9 | convolution fusion | flops 151412736 | bytes 4976768 | tf_op jit(solution)/shard_map/dot_general | solution.py:81
  15.4 0.2 copy.48
  15.6 0.0 copy-start.4
  15.6 0.0 copy-start.5
  15.6 0.3 fusion.44
  15.9 0.0 copy-done
  15.9 0.3 convolution_bitcast_fusion
  16.2 0.1 copy-done.4
  16.3 0.0 copy-done.5
  16.3 0.2 cosine_multiply_fusion
  16.5 0.0 copy-start.3
  16.5 0.8 fusion.43
  17.3 0.0 copy-start.7
  17.3 0.1 copy-done.3
  17.4 0.8 fusion.2
  18.3 0.1 copy.49
  18.4 0.0 copy-start.2
  18.4 3.3 %convolution_convert_fusion.2 = bf16[32,3072]{1,0:T(8,128)(2,1)S(1)} fusion(bf16[768,3072]{1,0:T(8,128)(2,1)} %param.27, f32[32,768]{1,0:T(8,128)S(1)} %copy.49, bf16[32,768]{1,0:T(8,128)(2,1)S(1)} %convolution_convert_fusion.3, f32[768]{0:T(1024)S(1)} %copy-done.7), kind=kOutput, calls=%fused_computation.2 | convolution fusion | flops 151388160 | bytes 5065728 | tf_op jit(solution)/shard_map/dot_general | solution.py:85
  21.7 2.3 %all-gather = bf16[64,3072]{1,0:T(8,128)(2,1)S(1)} all-gather(bf16[32,3072]{1,0:T(8,128)(2,1)S(1)} %convolution_convert_fusion.2), channel_id=2, replica_groups=mesh['ep'=16,'tp'=2] {'tp'}, dimensions={0}, use_global_device_ids=true | all-gather | bytes 589824 | tf_op jit(solution)/shard_map/all_gather | solution.py:12
  24.0 0.1 reduce_sum.69
  24.2 0.2 fusion.6
  24.4 0.1 convert_reduce_fusion.1
  24.5 0.4 convolution_convert_fusion.1
  24.9 0.2 broadcast_in_dim.2
  25.1 45.9 %all_to_all.10 = bf16[16,16,3072]{2,1,0:T(8,128)(2,1)S(1)} all-to-all(bf16[16,16,3072]{2,1,0:T(8,128)(2,1)S(1)} %bitcast.28), channel_id=1, replica_groups=mesh['ep'=16,'tp'=2] {'ep'}, dimensions={0} | all-to-all | bytes 3145728 | tf_op jit(solution)/shard_map/all_to_all | solution.py:110
  71.0 6.8 %fusion.45 = f32[256,1344]{0,1:T(8,128)} fusion(bf16[256,3072]{1,0:T(8,128)(2,1)S(1)} %bitcast.32, bf16[3072,1344]{0,1:T(8,128)(2,1)} %param.31), kind=kOutput, calls=%fused_computation.74 | convolution fusion | flops 2113929216 | bytes 11206656 | tf_op jit(solution)/shard_map/dot_general | solution.py:113
  77.7 16.3 %convolution_convert_fusion = bf16[256,3072]{1,0:T(8,128)(2,1)} fusion(bf16[1344,3072]{1,0:T(8,128)(2,1)} %param.33, bf16[256,3072]{1,0:T(8,128)(2,1)S(1)} %bitcast.33, bf16[3072,1344]{0,1:T(8,128)(2,1)} %param.32, f32[256,1344]{0,1:T(8,128)} %fusion.45), kind=kOutput, calls=%fused_computation | convolution fusion | flops 4230709248 | bytes 21037056 | tf_op jit(solution)/shard_map/dot_general | solution.py:116
  94.1 0.0 reduce-scatter.2.cloned.1.call-update
  94.1 7.4 %reduce-scatter.2.cloned.1.call-done = bf16[16,16,1536]{2,1,0:T(8,128)(2,1)} async-done(((bf16[16,16,3072]{2,1,0:T(8,128)(2,1)}), bf16[16,16,1536]{2,1,0:T(8,128)(2,1)}) %reduce-scatter.2.cloned.1.call-update) | async-done | bytes 786448 | tf_op jit(solution)/shard_map/reduce_scatter | solution.py:118
  101.5 6.9 %all-to-all-start.1 = ((bf16[16,16,1536]{2,1,0:T(8,128)(2,1)}), bf16[16,16,1536]{2,1,0:T(8,128)(2,1)S(1)}, u32[]{:S(2)}, u32[]{:S(2)}) async-start(bf16[16,16,1536]{2,1,0:T(8,128)(2,1)} %reduce-scatter.2.cloned.1.call-done), calls=%async_computation.2 | async-start | bytes 1572864 | tf_op jit(solution)/shard_map/all_to_all | solution.py:121
  108.4 0.3 pad_maximum_fusion
  108.7 1.3 copy.52
  110.1 18.4 %all-to-all-done.1 = bf16[16,16,1536]{2,1,0:T(8,128)(2,1)S(1)} async-done(((bf16[16,16,1536]{2,1,0:T(8,128)(2,1)}), bf16[16,16,1536]{2,1,0:T(8,128)(2,1)S(1)}, u32[]{:S(2)}, u32[]{:S(2)}) %all-to-all-start.1) | async-done | bytes 786464 | tf_op jit(solution)/shard_map/all_to_all | solution.py:121
  128.4 0.1 convert_reduce_fusion
  128.6 1.2 fusion.1
  (9 shorter events, 0.0 us)
Async XLA Ops:
  7.2 8.7 %copy-start = (bf16[48,128,16]{1,2,0:T(8,128)(2,1)S(1)}, bf16[48,128,16]{1,2,0:T(8,128)(2,1)}, u32[]{:S(2)}) copy-start(bf16[48,128,16]{1,2,0:T(8,128)(2,1)} %param.22) | copy-start | bytes 589828
  7.2 94.3 %reduce-scatter.2.cloned.1.call-start = ((), (), s32[]{:S(2)}) async-start(), calls=%async_computation.3 | async-start | bytes 2359296 | tf_op jit(solution)/shard_map/reduce_scatter | solution.py:118
  11.9 3.7 %copy-start.1 = (f32[32,48,128]{2,1,0:T(8,128)S(1)}, f32[32,48,128]{2,1,0:T(8,128)}, u32[]{:S(2)}) copy-start(f32[32,48,128]{2,1,0:T(8,128)} %param.18) | copy-start | bytes 2359300
  15.6 0.7 copy-start.4
  15.6 0.7 copy-start.5
  16.5 0.9 copy-start.3
  17.3 1.1 copy-start.7
  18.4 5.7 %copy-start.2 = (bf16[32,3072]{1,0:T(8,128)(2,1)S(1)}, bf16[32,3072]{1,0:T(8,128)(2,1)}, u32[]{:S(2)}) copy-start(bf16[32,3072]{1,0:T(8,128)(2,1)} %param.17) | copy-start | bytes 589828
  21.7 2.8 %copy-start.6 = (f32[3072]{0:T(1024)S(1)}, f32[3072]{0:T(1024)}, u32[]{:S(2)}) copy-start(f32[3072]{0:T(1024)} %param.28) | copy-start | bytes 36868
  101.5 26.9 %all-to-all-start.1 = ((bf16[16,16,1536]{2,1,0:T(8,128)(2,1)}), bf16[16,16,1536]{2,1,0:T(8,128)(2,1)S(1)}, u32[]{:S(2)}, u32[]{:S(2)}) async-start(bf16[16,16,1536]{2,1,0:T(8,128)(2,1)} %reduce-scatter.2.cloned.1.call-done), calls=%async_computation.2 | async-start | bytes 1572864 | tf_op jit(solution)/shard_map/all_to_all | solution.py:121
Sparse Core Ops, SparseCore 0:
  94.2 7.2 reduce-scatter.1
